TPU v7x, 32 devices: a whole 2x2x4 slice. The times are simulated.
32 devices in a mesh: fs: 8 (over z, y), tp: 4 (over x, core).
Axes of the slice: x: 2, y: 2, z: 4, core: 2. Of those that a mesh axis runs over, the one named last changes fastest.
Arguments:
- stream_in: bfloat16 [2048, 2112], P('fs'), may hold values from -6 to 6
- norm_gains: float32 [6, 2112], replicated, may hold values from 0.1 to 1.9
- gate_proj: bfloat16 [2112, 3072], P('fs', 'tp'), may hold values from -0.125 to 0.125
- up_proj: bfloat16 [2112, 3072], P('fs', 'tp'), may hold values from -0.125 to 0.125
- down_proj: bfloat16 [2112, 3072], P('fs', 'tp'), may hold values from -0.109375 to 0.109375
- outer_gate: bfloat16 [2112, 1056], P('fs', 'tp'), may hold values from -0.125 to 0.125
- inner_gate: bfloat16 [2112, 1056], P('fs', 'tp'), may hold values from -0.125 to 0.125
- value_proj: bfloat16 [2112, 1056], P('fs', 'tp'), may hold values from -0.125 to 0.125
- mixer_out: bfloat16 [2112, 1056], P('fs', 'tp'), may hold values from -0.1875 to 0.1875
- conv_taps: bfloat16 [3, 1056], replicated, may hold values from -3 to 3
Outputs:
- stream_out: bfloat16 [2048, 2112], P('fs')
All inputs are finite; a program needn't handle non-finite values.
Results may differ from a plain program's by a relative error of at most 0.02.
Values may be sent and summed in bfloat16 or wider, within the bound.
A program may use at most 64 MiB of HBM per device.

v0:
```python
import jax
import jax.numpy as jnp
from jax import lax
from jax.sharding import PartitionSpec as P

CONV_K = 3
EPSILON = 1e-06


def scaled(values, gain):
    return values * lax.rsqrt(jnp.mean(values * values, axis=-1, keepdims=True) + EPSILON) * gain


def narrow(inner, weight, stream, gain, factor):
    partial_value = lax.dot_general(
        inner, weight, (((1,), (1,)), ((), ())), preferred_element_type=jnp.float32
    )
    summed = lax.psum(partial_value.astype(jnp.bfloat16), "tp").astype(jnp.float32)
    return (stream.astype(jnp.float32) + factor * scaled(summed, gain)).astype(jnp.bfloat16)


def half_step(stream, weights, pre_gain, post_gain):
    gate_full, up_full, down_full = weights
    normed = scaled(stream.astype(jnp.float32), pre_gain).astype(jnp.bfloat16)
    gate = jnp.dot(normed, gate_full, preferred_element_type=jnp.float32)
    upward = jnp.dot(normed, up_full, preferred_element_type=jnp.float32)
    hidden = (jax.nn.silu(gate) * upward).astype(jnp.bfloat16)
    return narrow(hidden, down_full, stream, post_gain, 0.5)


def mixer_step(stream, weights, conv_taps, pre_gain, post_gain):
    outer_full, inner_full, value_full, out_full = weights
    channels = outer_full.shape[1]
    normed = scaled(stream.astype(jnp.float32), pre_gain).astype(jnp.bfloat16)
    outer = (
        jnp.dot(normed, outer_full, preferred_element_type=jnp.float32)
        .astype(jnp.bfloat16)
        .astype(jnp.float32)
    )
    inner = (
        jnp.dot(normed, inner_full, preferred_element_type=jnp.float32)
        .astype(jnp.bfloat16)
        .astype(jnp.float32)
    )
    value = (
        jnp.dot(normed, value_full, preferred_element_type=jnp.float32)
        .astype(jnp.bfloat16)
        .astype(jnp.float32)
    )
    gated = inner * value
    taps = lax.dynamic_slice_in_dim(conv_taps, lax.axis_index("tp") * channels, channels, 1).astype(
        jnp.float32
    )
    length = gated.shape[0]
    padded = jnp.concatenate([jnp.zeros((CONV_K - 1, channels), jnp.float32), gated], axis=0)
    conv = jnp.zeros_like(gated)
    for offset in range(CONV_K):
        conv = conv + taps[offset] * padded[offset : offset + length]
    mixed = (outer * conv).astype(jnp.bfloat16)
    return narrow(mixed, out_full, stream, post_gain, 1.0)


def local(
    stream_in,
    norm_gains,
    gate_proj,
    up_proj,
    down_proj,
    outer_gate,
    inner_gate,
    value_proj,
    mixer_out,
    conv_taps,
):
    mlp_full = (
        lax.all_gather(gate_proj, "fs", axis=0, tiled=True),
        lax.all_gather(up_proj, "fs", axis=0, tiled=True),
        lax.all_gather(down_proj, "fs", axis=0, tiled=True),
    )
    mixer_full = None
    stream = half_step(stream_in, mlp_full, norm_gains[0], norm_gains[1])
    mixer_full = (
        lax.all_gather(outer_gate, "fs", axis=0, tiled=True),
        lax.all_gather(inner_gate, "fs", axis=0, tiled=True),
        lax.all_gather(value_proj, "fs", axis=0, tiled=True),
        lax.all_gather(mixer_out, "fs", axis=0, tiled=True),
    )
    stream = mixer_step(stream, mixer_full, conv_taps, norm_gains[2], norm_gains[3])
    return half_step(stream, mlp_full, norm_gains[4], norm_gains[5])


def solution(mesh):
    return jax.shard_map(
        local,
        mesh=mesh,
        in_specs=(
            P("fs", None),
            P(),
            P("fs", "tp"),
            P("fs", "tp"),
            P("fs", "tp"),
            P("fs", "tp"),
            P("fs", "tp"),
            P("fs", "tp"),
            P("fs", "tp"),
            P(),
        ),
        out_specs=P("fs", None),
        check_vma=False,
    )
```

profile of v0, /device:TPU:0, one launch (start us, length us, event | category | flops | bytes accessed | tf_op | source)
XLA Modules:
  0.0 522.5 jit_solution(16457004554758750413)
XLA Ops:
  6.5 0.0 all-gather.8.cloned.1.call-start
  6.5 0.7 all-gather.8.cloned.1.call-update
  7.3 0.0 all-gather.10.cloned.1.call-start
  7.3 0.7 all-gather.10.cloned.1.call-update
  8.0 0.0 all-gather.12.cloned.1.call-start
  8.1 0.7 all-gather.12.cloned.1.call-update
  8.7 0.0 all-reduce.5.cloned.1.call-start
  8.8 1.4 slice_reduce_fusion
  10.2 1.6 fusion.8
  11.8 61.5 %all-gather.8.cloned.1.call-done = bf16[2112,768]{1,0:T(8,128)(2,1)} async-done(((bf16[264,768]{1,0:T(8,128)(2,1)}), bf16[2112,768]{1,0:T(8,128)(2,1)}) %all-gather.8.cloned.1.call-update) | async-done | bytes 3244048 | tf_op jit(solution)/shard_map/all_gather | solution.py:76
  73.3 0.0 copy-done
  73.3 3.2 fusion.36
  76.6 58.7 %all-gather.10.cloned.1.call-done = bf16[2112,768]{1,0:T(8,128)(2,1)} async-done(((bf16[264,768]{1,0:T(8,128)(2,1)}), bf16[2112,768]{1,0:T(8,128)(2,1)}) %all-gather.10.cloned.1.call-update) | async-done | bytes 3244048 | tf_op jit(solution)/shard_map/all_gather | solution.py:77
  135.3 62.0 %all-gather.12.cloned.1.call-done = bf16[2112,768]{1,0:T(8,128)(2,1)} async-done(((bf16[264,768]{1,0:T(8,128)(2,1)}), bf16[2112,768]{1,0:T(8,128)(2,1)}) %all-gather.12.cloned.1.call-update) | async-done | bytes 3244048 | tf_op jit(solution)/shard_map/all_gather | solution.py:78
  197.2 6.6 %convolution_convert_fusion.2 = bf16[256,2112]{0,1:T(8,128)(2,1)} fusion(bf16[2112,768]{1,0:T(8,128)(2,1)} %all-gather.12.cloned.1.call-done, bf16[2112,768]{1,0:T(8,128)(2,1)} %all-gather.10.cloned.1.call-done, f32[256,768]{1,0:T(8,128)S(1)} %fusion.36, bf16[256,2112]{0,1:T(8,128)(2,1)S(1)} %copy-done, f32[2112]{0:T(1024)S(1)} %get-tuple-element.9, ...), kind=kOutput, calls=%fused_computation.2 | convolution fusion | flops 1664827392 | bytes 9446656 | tf_op jit(solution)/shard_map/dot_general | solution.py:15
  203.9 0.0 all-reduce.5.cloned.1.call-update
  203.9 0.0 all-gather.16.cloned.1.call-start
  203.9 0.5 all-gather.16.cloned.1.call-update
  204.5 0.0 all-gather.18.cloned.1.call-start
  204.5 0.5 all-gather.18.cloned.1.call-update
  205.0 0.0 all-gather.14.cloned.1.call-start
  205.1 0.7 all-gather.14.cloned.1.call-update
  205.8 0.0 all-gather.20.cloned.1.call-start
  205.8 0.7 all-gather.20.cloned.1.call-update
  206.5 0.0 all-reduce.7.cloned.1.call-start
  206.6 0.8 dynamic-slice_convert_fusion
  207.4 32.0 %all-reduce.5.cloned.1.call-done = bf16[256,2112]{0,1:T(8,128)(2,1)} async-done(((bf16[256,2112]{0,1:T(8,128)(2,1)}), bf16[256,2112]{0,1:T(8,128)(2,1)}) %all-reduce.5.cloned.1.call-update) | async-done | bytes 1081360 | tf_op jit(solution)/shard_map/psum | solution.py:18
  239.4 1.5 fusion
  241.0 1.9 fusion.12
  242.9 43.7 %all-gather.16.cloned.1.call-done = bf16[2112,264]{1,0:T(8,128)(2,1)} async-done(((bf16[264,264]{1,0:T(8,128)(2,1)}), bf16[2112,264]{1,0:T(8,128)(2,1)}) %all-gather.16.cloned.1.call-update) | async-done | bytes 1115152 | tf_op jit(solution)/shard_map/all_gather | solution.py:84
  286.6 2.5 fusion.24
  289.0 42.7 %all-gather.18.cloned.1.call-done = bf16[2112,264]{1,0:T(8,128)(2,1)} async-done(((bf16[264,264]{1,0:T(8,128)(2,1)}), bf16[2112,264]{1,0:T(8,128)(2,1)}) %all-gather.18.cloned.1.call-update) | async-done | bytes 1115152 | tf_op jit(solution)/shard_map/all_gather | solution.py:85
  331.7 2.5 fusion.23
  334.2 42.9 %all-gather.14.cloned.1.call-done = bf16[2112,264]{1,0:T(8,128)(2,1)} async-done(((bf16[264,264]{1,0:T(8,128)(2,1)}), bf16[2112,264]{1,0:T(8,128)(2,1)}) %all-gather.14.cloned.1.call-update) | async-done | bytes 1115152 | tf_op jit(solution)/shard_map/all_gather | solution.py:83
  377.1 45.3 %all-gather.20.cloned.1.call-done = bf16[2112,264]{1,0:T(8,128)(2,1)} async-done(((bf16[264,264]{1,0:T(8,128)(2,1)}), bf16[2112,264]{1,0:T(8,128)(2,1)}) %all-gather.20.cloned.1.call-update) | async-done | bytes 1115152 | tf_op jit(solution)/shard_map/all_gather | solution.py:86
  422.4 5.0 convolution_convert_fusion.1
  427.4 0.0 all-reduce.7.cloned.1.call-update
  427.4 0.2 all-reduce.9.cloned.1.call-start
  427.6 35.0 %all-reduce.7.cloned.1.call-done = bf16[256,2112]{0,1:T(8,128)(2,1)} async-done(((bf16[256,2112]{0,1:T(8,128)(2,1)}), bf16[256,2112]{0,1:T(8,128)(2,1)}) %all-reduce.7.cloned.1.call-update) | async-done | bytes 1081360 | tf_op jit(solution)/shard_map/psum | solution.py:18
  462.6 1.7 fusion.3
  464.3 1.8 fusion.16
  466.1 0.0 copy-done.1
  466.1 1.4 fusion.32
  467.5 6.6 %convolution_convert_fusion = bf16[256,2112]{0,1:T(8,128)(2,1)} fusion(bf16[2112,768]{1,0:T(8,128)(2,1)} %all-gather.12.cloned.1.call-done, bf16[2112,768]{1,0:T(8,128)(2,1)} %all-gather.10.cloned.1.call-done, f32[256,768]{1,0:T(8,128)S(1)} %fusion.32, bf16[256,2112]{0,1:T(8,128)(2,1)S(1)} %get-tuple-element.15, f32[2112]{0:T(1024)S(1)} %get-tuple-element.10, ...), kind=kOutput, calls=%fused_computation | convolution fusion | flops 1664827392 | bytes 9446656 | tf_op jit(solution)/shard_map/dot_general | solution.py:15
  474.1 0.0 all-reduce.9.cloned.1.call-update
  474.1 37.2 %all-reduce.9.cloned.1.call-done = bf16[256,2112]{0,1:T(8,128)(2,1)} async-done(((bf16[256,2112]{0,1:T(8,128)(2,1)}), bf16[256,2112]{0,1:T(8,128)(2,1)}) %all-reduce.9.cloned.1.call-update) | async-done | bytes 1081360 | tf_op jit(solution)/shard_map/psum | solution.py:18
  511.3 1.5 fusion.5
  512.9 2.7 fusion.19
  (9 shorter events, 0.1 us)
Async XLA Ops:
  6.5 66.8 %copy-start = (bf16[256,2112]{0,1:T(8,128)(2,1)S(1)}, bf16[256,2112]{0,1:T(8,128)(2,1)}, u32[]{:S(2)}) copy-start(bf16[256,2112]{0,1:T(8,128)(2,1)} %param.10) | copy-start | bytes 3244036
  6.5 66.8 %all-gather.8.cloned.1.call-start = ((), (), s32[]{:S(2)}) async-start(), calls=%async_computation | async-start | bytes 3649536 | tf_op jit(solution)/shard_map/all_gather | solution.py:76
  7.3 128.0 %all-gather.10.cloned.1.call-start = ((), (), s32[]{:S(2)}) async-start(), calls=%async_computation.1 | async-start | bytes 3649536 | tf_op jit(solution)/shard_map/all_gather | solution.py:77
  8.0 189.2 %all-gather.12.cloned.1.call-start = ((), (), s32[]{:S(2)}) async-start(), calls=%async_computation.2 | async-start | bytes 3649536 | tf_op jit(solution)/shard_map/all_gather | solution.py:78
  8.7 230.7 %all-reduce.5.cloned.1.call-start = ((), (), s32[]{:S(2)}) async-start(), calls=%async_computation.3 | async-start | bytes 2162688 | tf_op jit(solution)/shard_map/psum | solution.py:18
  203.9 82.7 %all-gather.16.cloned.1.call-start = ((), (), s32[]{:S(2)}) async-start(), calls=%async_computation.5 | async-start | bytes 1824768 | tf_op jit(solution)/shard_map/all_gather | solution.py:84
  204.5 127.3 %all-gather.18.cloned.1.call-start = ((), (), s32[]{:S(2)}) async-start(), calls=%async_computation.6 | async-start | bytes 1824768 | tf_op jit(solution)/shard_map/all_gather | solution.py:85
  205.0 172.0 %all-gather.14.cloned.1.call-start = ((), (), s32[]{:S(2)}) async-start(), calls=%async_computation.4 | async-start | bytes 1824768 | tf_op jit(solution)/shard_map/all_gather | solution.py:83
  205.8 216.6 %all-gather.20.cloned.1.call-start = ((), (), s32[]{:S(2)}) async-start(), calls=%async_computation.7 | async-start | bytes 1824768 | tf_op jit(solution)/shard_map/all_gather | solution.py:86
  206.5 256.0 %all-reduce.7.cloned.1.call-start = ((), (), s32[]{:S(2)}) async-start(), calls=%async_computation.8 | async-start | bytes 2162688 | tf_op jit(solution)/shard_map/psum | solution.py:18
  427.4 83.9 %all-reduce.9.cloned.1.call-start = ((), (), s32[]{:S(2)}) async-start(), calls=%async_computation.9 | async-start | bytes 2162688 | tf_op jit(solution)/shard_map/psum | solution.py:18
  462.6 3.6 copy-start.1
Sparse Core Ops, SparseCore 0:
  9.5 63.7 all-gather.7
  75.5 59.7 all-gather.9
  137.5 59.7 all-gather.11
  204.0 35.3 all-reduce.4
  241.4 45.0 all-gather.15
  288.6 43.0 all-gather.17
  333.9 43.0 all-gather.13
  379.3 43.0 all-gather.19
  427.5 35.0 all-reduce.6
  474.3 37.0 all-reduce.8
where the time goes:
time: 523 us; the launch traced here: 522 us
  waiting for transfers between devices  466 us (89%)
  matrix products  27.7 us (5%)
  other arithmetic  13.6 us (3%)
  between operations  13.6 us (3%)
    psum x3, waiting for transfers between devices, narrow(): lax.psum(partial_value.astype(jnp.bfloat16), 'tp').astype(jnp.float32)  104 us
    all_gather x1, waiting for transfers between devices, local(): lax.all_gather(down_proj, 'fs', axis=0, tiled=True)  62 us
    all_gather x1, waiting for transfers between devices, local(): lax.all_gather(gate_proj, 'fs', axis=0, tiled=True)  61.5 us
    all_gather x1, waiting for transfers between devices, local(): lax.all_gather(up_proj, 'fs', axis=0, tiled=True)  58.7 us
    all_gather x1, waiting for transfers between devices, local(): lax.all_gather(mixer_out, 'fs', axis=0, tiled=True)  45.3 us
    all_gather x1, waiting for transfers between devices, local(): lax.all_gather(inner_gate, 'fs', axis=0, tiled=True)  43.7 us
    all_gather x1, waiting for transfers between devices, local(): lax.all_gather(outer_gate, 'fs', axis=0, tiled=True)  42.9 us
    all_gather x1, waiting for transfers between devices, local(): lax.all_gather(value_proj, 'fs', axis=0, tiled=True)  42.7 us
  transfers between devices with their start and end apart: 10, of which 10 were waited for; matrix products, arithmetic and copies ran while one was open for 3% of the time, Pallas kernels for 0%

commit v1 on v0

--- a/solution.py
+++ b/solution.py
@@ -15,7 +15,9 @@
     partial_value = lax.dot_general(
         inner, weight, (((1,), (1,)), ((), ())), preferred_element_type=jnp.float32
     )
-    summed = lax.psum(partial_value.astype(jnp.bfloat16), "tp").astype(jnp.float32)
+    summed = jnp.sum(lax.all_gather(partial_value.astype(jnp.bfloat16), "tp"), axis=0).astype(
+        jnp.float32
+    )
     return (stream.astype(jnp.float32) + factor * scaled(summed, gain)).astype(jnp.bfloat16)
 
 

time: 523 us -> 557 us (1.065)
  local copies, waits for them, and re-layouts: 1.48 us -> 29.2 us
  other arithmetic: 13.6 us -> 40.6 us
  waiting for transfers between devices: 466 us -> 444 us
    psum x3 -> x0, waiting for transfers between devices: 104 us -> none  [narrow(): lax.psum(partial_value.astype(jnp.bfloat16), 'tp').astype(jnp.float32)]
    all_gather x0 -> x3, waiting for transfers between devices: none -> 101 us  [narrow(): lax.all_gather(partial_value.astype(jnp.bfloat16), 'tp')]
    reduce_sum x0 -> x3, other arithmetic: none -> 34.5 us  [narrow(): jnp.sum(lax.all_gather(partial_value.astype(jnp.bfloat16), 'tp'), axis=0)]
    all_gather x0 -> x3, local copies, waits for them, and re-layouts: none -> 26.8 us  [narrow(): lax.all_gather(partial_value.astype(jnp.bfloat16), 'tp')]
    all_gather x1, waiting for transfers between devices: 43.7 us -> 25.4 us  [local(): lax.all_gather(inner_gate, 'fs', axis=0, tiled=True)]
    reduce_sum x6, other arithmetic: 10.1 us -> 3.73 us  [scaled(): jnp.mean(values * values, axis=-1, keepdims=True) + EPSILON]
  transfers between devices with their start and end apart: 10 -> 10, of which waited for: 10 -> 10; matrix products, arithmetic and copies ran while one was open for 3% -> 6% of each run, Pallas kernels for 0% -> 0%
where the time goes in v1:
time: 557 us; the launch traced here: 556 us
  waiting for transfers between devices  444 us (80%)
  other arithmetic  40.6 us (7%)
  local copies, waits for them, and re-layouts  29.2 us (5%)
  matrix products  27.6 us (5%)
  between operations  13.6 us (2%)
    all_gather x3, waiting for transfers between devices, narrow(): lax.all_gather(partial_value.astype(jnp.bfloat16), 'tp')  101 us
    all_gather x1, waiting for transfers between devices, local(): lax.all_gather(down_proj, 'fs', axis=0, tiled=True)  62 us
    all_gather x1, waiting for transfers between devices, local(): lax.all_gather(gate_proj, 'fs', axis=0, tiled=True)  61.5 us
    all_gather x1, waiting for transfers between devices, local(): lax.all_gather(up_proj, 'fs', axis=0, tiled=True)  58.7 us
    all_gather x1, waiting for transfers between devices, local(): lax.all_gather(mixer_out, 'fs', axis=0, tiled=True)  45.3 us
    all_gather x1, waiting for transfers between devices, local(): lax.all_gather(outer_gate, 'fs', axis=0, tiled=True)  42.9 us
    all_gather x1, waiting for transfers between devices, local(): lax.all_gather(value_proj, 'fs', axis=0, tiled=True)  42.7 us
    reduce_sum x3, other arithmetic, narrow(): jnp.sum(lax.all_gather(partial_value.astype(jnp.bfloat16), 'tp'), axis=0)  34.5 us
  transfers between devices with their start and end apart: 10, of which 10 were waited for; matrix products, arithmetic and copies ran while one was open for 6% of the time, Pallas kernels for 0%

profile of v1, /device:TPU:0, one launch (start us, length us, event | category | flops | bytes accessed | tf_op | source)
XLA Modules:
  0.0 555.7 jit_solution(5127036367963951343)
XLA Ops:
  6.5 0.7 all-gather.14.cloned.1.call-update
  7.3 0.0 all-gather.16.cloned.1.call-start
  7.3 0.7 all-gather.16.cloned.1.call-update
  8.0 0.0 all-gather.18.cloned.1.call-start
  8.1 0.7 all-gather.18.cloned.1.call-update
  8.7 0.0 all-gather.28.cloned.1.call-start
  8.8 1.5 slice_reduce_fusion
  10.2 1.6 fusion.8
  11.8 61.5 %all-gather.14.cloned.1.call-done = bf16[2112,768]{1,0:T(8,128)(2,1)} async-done(((bf16[264,768]{1,0:T(8,128)(2,1)}), bf16[2112,768]{1,0:T(8,128)(2,1)}) %all-gather.14.cloned.1.call-update) | async-done | bytes 3244048 | tf_op jit(solution)/shard_map/all_gather | solution.py:78
  73.3 3.2 fusion.36
  76.5 58.7 %all-gather.16.cloned.1.call-done = bf16[2112,768]{1,0:T(8,128)(2,1)} async-done(((bf16[264,768]{1,0:T(8,128)(2,1)}), bf16[2112,768]{1,0:T(8,128)(2,1)}) %all-gather.16.cloned.1.call-update) | async-done | bytes 3244048 | tf_op jit(solution)/shard_map/all_gather | solution.py:79
  135.3 62.0 %all-gather.18.cloned.1.call-done = bf16[2112,768]{1,0:T(8,128)(2,1)} async-done(((bf16[264,768]{1,0:T(8,128)(2,1)}), bf16[2112,768]{1,0:T(8,128)(2,1)}) %all-gather.18.cloned.1.call-update) | async-done | bytes 3244048 | tf_op jit(solution)/shard_map/all_gather | solution.py:80
  197.2 6.6 %convolution_convert_fusion.2 = bf16[256,2112]{0,1:T(8,128)(2,1)} fusion(bf16[2112,768]{1,0:T(8,128)(2,1)} %all-gather.18.cloned.1.call-done, bf16[2112,768]{1,0:T(8,128)(2,1)} %all-gather.16.cloned.1.call-done, f32[256,768]{1,0:T(8,128)S(1)} %fusion.36, bf16[256,2112]{0,1:T(8,128)(2,1)S(1)} %copy-done, f32[2112]{0:T(1024)S(1)} %get-tuple-element.9, ...), kind=kOutput, calls=%fused_computation.2 | convolution fusion | flops 1664827392 | bytes 9446656 | tf_op jit(solution)/shard_map/dot_general | solution.py:15
  203.9 0.0 all-gather.22.cloned.1.call-start
  203.9 0.5 all-gather.22.cloned.1.call-update
  204.5 0.0 all-gather.24.cloned.1.call-start
  204.5 0.5 all-gather.24.cloned.1.call-update
  205.0 0.0 all-gather.20.cloned.1.call-start
  205.1 0.7 all-gather.20.cloned.1.call-update
  205.8 0.7 all-gather.26.cloned.1.call-update
  206.5 0.2 all-gather.30.cloned.1.call-start
  206.8 0.8 dynamic-slice_convert_fusion
  207.6 30.9 %all-gather.28.cloned.1.call-done = bf16[1024,2112]{0,1:T(8,128)(2,1)} async-done(((bf16[256,2112]{0,1:T(8,128)(2,1)}), bf16[1024,2112]{0,1:T(8,128)(2,1)}) %all-gather.28.cloned.1.call-update) | async-done | bytes 4325392 | tf_op jit(solution)/shard_map/all_gather | solution.py:18
  238.5 8.9 %reshape.48 = bf16[4,256,2112]{1,0,2:T(4,128)(2,1)} reshape(bf16[1024,2112]{0,1:T(8,128)(2,1)} %all-gather.28.cloned.1.call-done) | data formatting | bytes 8650752 | tf_op jit(solution)/shard_map/all_gather | solution.py:18
  247.4 11.5 %reduce_sum.91 = bf16[256,2112]{0,1:T(8,128)(2,1)S(1)} reduce(bf16[4,256,2112]{1,0,2:T(4,128)(2,1)} %reshape.48, bf16[]{:T(256)} %constant.27.clone.1), dimensions={0}, to_apply=%region_1.2 | reduce | flops 1622016 | bytes 5406722 | tf_op jit(solution)/shard_map/reduce_sum | solution.py:18
  258.9 0.3 fusion
  259.2 0.7 fusion.12
  259.9 25.4 %all-gather.22.cloned.1.call-done = bf16[2112,264]{1,0:T(8,128)(2,1)} async-done(((bf16[264,264]{1,0:T(8,128)(2,1)}), bf16[2112,264]{1,0:T(8,128)(2,1)}) %all-gather.22.cloned.1.call-update) | async-done | bytes 1115152 | tf_op jit(solution)/shard_map/all_gather | solution.py:86
  285.3 2.4 fusion.24
  287.7 42.7 %all-gather.24.cloned.1.call-done = bf16[2112,264]{1,0:T(8,128)(2,1)} async-done(((bf16[264,264]{1,0:T(8,128)(2,1)}), bf16[2112,264]{1,0:T(8,128)(2,1)}) %all-gather.24.cloned.1.call-update) | async-done | bytes 1115152 | tf_op jit(solution)/shard_map/all_gather | solution.py:87
  330.5 2.4 fusion.23
  332.9 42.9 %all-gather.20.cloned.1.call-done = bf16[2112,264]{1,0:T(8,128)(2,1)} async-done(((bf16[264,264]{1,0:T(8,128)(2,1)}), bf16[2112,264]{1,0:T(8,128)(2,1)}) %all-gather.20.cloned.1.call-update) | async-done | bytes 1115152 | tf_op jit(solution)/shard_map/all_gather | solution.py:85
  375.8 45.3 %all-gather.26.cloned.1.call-done = bf16[2112,264]{1,0:T(8,128)(2,1)} async-done(((bf16[264,264]{1,0:T(8,128)(2,1)}), bf16[2112,264]{1,0:T(8,128)(2,1)}) %all-gather.26.cloned.1.call-update) | async-done | bytes 1115152 | tf_op jit(solution)/shard_map/all_gather | solution.py:88
  421.1 4.9 convolution_convert_fusion.1
  426.1 0.0 all-gather.32.cloned.1.call-start
  426.1 34.2 %all-gather.30.cloned.1.call-done = bf16[1024,2112]{0,1:T(8,128)(2,1)} async-done(((bf16[256,2112]{0,1:T(8,128)(2,1)}), bf16[1024,2112]{0,1:T(8,128)(2,1)}) %all-gather.30.cloned.1.call-update) | async-done | bytes 4325392 | tf_op jit(solution)/shard_map/all_gather | solution.py:18
  460.3 8.9 %reshape.49 = bf16[4,256,2112]{1,0,2:T(4,128)(2,1)} reshape(bf16[1024,2112]{0,1:T(8,128)(2,1)} %all-gather.30.cloned.1.call-done) | data formatting | bytes 8650752 | tf_op jit(solution)/shard_map/all_gather | solution.py:18
  469.3 11.5 %reduce_sum.94 = bf16[256,2112]{0,1:T(8,128)(2,1)S(1)} reduce(bf16[4,256,2112]{1,0,2:T(4,128)(2,1)} %reshape.49, bf16[]{:T(256)} %constant.27.clone.1), dimensions={0}, to_apply=%region_4.5 | reduce | flops 1622016 | bytes 5406722 | tf_op jit(solution)/shard_map/reduce_sum | solution.py:18
  480.8 0.3 fusion.3
  481.1 0.6 fusion.16
  481.7 1.0 copy-done.1
  482.7 1.4 fusion.32
  484.0 6.6 %convolution_convert_fusion = bf16[256,2112]{0,1:T(8,128)(2,1)} fusion(bf16[2112,768]{1,0:T(8,128)(2,1)} %all-gather.18.cloned.1.call-done, bf16[2112,768]{1,0:T(8,128)(2,1)} %all-gather.16.cloned.1.call-done, f32[256,768]{1,0:T(8,128)S(1)} %fusion.32, bf16[256,2112]{0,1:T(8,128)(2,1)S(1)} %get-tuple-element.15, f32[2112]{0:T(1024)S(1)} %get-tuple-element.10, ...), kind=kOutput, calls=%fused_computation | convolution fusion | flops 1664827392 | bytes 9446656 | tf_op jit(solution)/shard_map/dot_general | solution.py:15
  490.7 35.9 %all-gather.32.cloned.1.call-done = bf16[1024,2112]{0,1:T(8,128)(2,1)} async-done(((bf16[256,2112]{0,1:T(8,128)(2,1)}), bf16[1024,2112]{0,1:T(8,128)(2,1)}) %all-gather.32.cloned.1.call-update) | async-done | bytes 4325392 | tf_op jit(solution)/shard_map/all_gather | solution.py:18
  526.6 8.9 %reshape.50 = bf16[4,256,2112]{1,0,2:T(4,128)(2,1)} reshape(bf16[1024,2112]{0,1:T(8,128)(2,1)} %all-gather.32.cloned.1.call-done) | data formatting | bytes 8650752 | tf_op jit(solution)/shard_map/all_gather | solution.py:18
  535.5 11.5 %reduce_sum.97 = bf16[256,2112]{0,1:T(8,128)(2,1)S(1)} reduce(bf16[4,256,2112]{1,0,2:T(4,128)(2,1)} %reshape.50, bf16[]{:T(256)} %constant.27.clone.1), dimensions={0}, to_apply=%region_7.8 | reduce | flops 1622016 | bytes 5406722 | tf_op jit(solution)/shard_map/reduce_sum | solution.py:18
  547.0 0.3 fusion.5
  547.4 1.5 fusion.19
  (15 shorter events, 0.2 us)
Async XLA Ops:
  6.5 66.8 %copy-start = (bf16[256,2112]{0,1:T(8,128)(2,1)S(1)}, bf16[256,2112]{0,1:T(8,128)(2,1)}, u32[]{:S(2)}) copy-start(bf16[256,2112]{0,1:T(8,128)(2,1)} %param.10) | copy-start | bytes 3244036
  6.5 66.8 %all-gather.14.cloned.1.call-start = ((), (), s32[]{:S(2)}) async-start(), calls=%async_computation | async-start | bytes 3649536 | tf_op jit(solution)/shard_map/all_gather | solution.py:78
  7.3 128.0 %all-gather.16.cloned.1.call-start = ((), (), s32[]{:S(2)}) async-start(), calls=%async_computation.1 | async-start | bytes 3649536 | tf_op jit(solution)/shard_map/all_gather | solution.py:79
  8.0 189.2 %all-gather.18.cloned.1.call-start = ((), (), s32[]{:S(2)}) async-start(), calls=%async_computation.2 | async-start | bytes 3649536 | tf_op jit(solution)/shard_map/all_gather | solution.py:80
  8.7 229.7 %all-gather.28.cloned.1.call-start = ((), (), s32[]{:S(2)}) async-start(), calls=%async_computation.7 | async-start | bytes 5406720 | tf_op jit(solution)/shard_map/all_gather | solution.py:18
  203.9 81.4 %all-gather.22.cloned.1.call-start = ((), (), s32[]{:S(2)}) async-start(), calls=%async_computation.4 | async-start | bytes 1824768 | tf_op jit(solution)/shard_map/all_gather | solution.py:86
  204.5 126.0 %all-gather.24.cloned.1.call-start = ((), (), s32[]{:S(2)}) async-start(), calls=%async_computation.5 | async-start | bytes 1824768 | tf_op jit(solution)/shard_map/all_gather | solution.py:87
  205.0 170.8 %all-gather.20.cloned.1.call-start = ((), (), s32[]{:S(2)}) async-start(), calls=%async_computation.3 | async-start | bytes 1824768 | tf_op jit(solution)/shard_map/all_gather | solution.py:85
  205.8 215.3 %all-gather.26.cloned.1.call-start = ((), (), s32[]{:S(2)}) async-start(), calls=%async_computation.6 | async-start | bytes 1824768 | tf_op jit(solution)/shard_map/all_gather | solution.py:88
  206.5 253.8 %all-gather.30.cloned.1.call-start = ((), (), s32[]{:S(2)}) async-start(), calls=%async_computation.8 | async-start | bytes 5406720 | tf_op jit(solution)/shard_map/all_gather | solution.py:18
  426.1 100.5 %all-gather.32.cloned.1.call-start = ((), (), s32[]{:S(2)}) async-start(), calls=%async_computation.9 | async-start | bytes 5406720 | tf_op jit(solution)/shard_map/all_gather | solution.py:18
  480.8 1.9 copy-start.1
Sparse Core Ops, SparseCore 0:
  9.5 63.7 all-gather.13
  75.5 59.7 all-gather.15
  137.4 59.7 all-gather.17
  204.0 34.4 all-gather.27
  240.5 44.7 all-gather.21
  287.3 43.0 all-gather.23
  332.7 43.0 all-gather.19
  378.0 43.0 all-gather.25
  426.2 34.0 all-gather.29
  490.8 35.7 all-gather.31
